TPU v7x, 32 devices: a whole 2x2x4 slice. The times are simulated.
32 devices in a mesh: fs: 8 (over z, y), tp: 4 (over x, core).
Axes of the slice: x: 2, y: 2, z: 4, core: 2. Of those that a mesh axis runs over, the one named last changes fastest.
Arguments:
- hidden_in: bfloat16 [2048, 2048], P('fs'), may hold values from -6 to 6
- mix_gain: float32 [2048], replicated, may hold values from 0.1 to 1.9
- value_proj: float32 [2048, 512], P('fs', 'tp'), may hold values from -0.125 to 0.125
- gate_proj: float32 [2048, 512], P('fs', 'tp'), may hold values from -0.125 to 0.125
- out_proj: float32 [2048, 512], P('fs', 'tp'), may hold values from -0.25 to 0.25
- value_scale: float32 [512], P('tp'), may hold values from 0.3 to 3
- gate_scale: float32 [512], P('tp'), may hold values from 0.5 to 2
- out_scale: float32 [2048], P('fs'), may hold values from 0.5 to 2
- conv_kernel: bfloat16 [31, 512], P(None, 'tp'), may hold values from -1 to 1
- norm_gain: float32 [512], P('tp'), may hold values from 0.1 to 1.9
- norm_shift: float32 [512], P('tp'), may hold values from -3 to 3
- mlp_gain: float32 [2048], replicated, may hold values from 0.1 to 1.9
- mlp_gate: float32 [2048, 2816], P('fs', 'tp'), may hold values from -0.125 to 0.125
- mlp_up: float32 [2048, 2816], P('fs', 'tp'), may hold values from -0.125 to 0.125
- mlp_down: float32 [2048, 2816], P('fs', 'tp'), may hold values from -0.109375 to 0.109375
- mlp_gate_scale: float32 [2816], P('tp'), may hold values from 0.5 to 2
- mlp_up_scale: float32 [2816], P('tp'), may hold values from 0.5 to 2
- mlp_down_scale: float32 [2048], P('fs'), may hold values from 0.5 to 2
Outputs:
- layer_out: bfloat16 [2048, 2048], P('fs')
All inputs are finite; a program needn't handle non-finite values.
Results may differ from a plain program's by a relative error of at most 0.019.
Values may be sent and summed in bfloat16 or wider, within the bound.
A program may use at most 64 MiB of HBM per device.

v0:
```python
import jax
import jax.numpy as jnp
from jax import lax
from jax.sharding import PartitionSpec as P


def row_norm(rows, gain):
    scale = lax.rsqrt(jnp.mean(rows * rows, axis=-1, keepdims=True) + 1e-06)
    return rows * scale * gain


def contract_last(left, right):
    return lax.dot_general(
        left, right, (((1,), (1,)), ((), ())), preferred_element_type=jnp.float32
    )


def body(
    hidden_in,
    mix_gain,
    value_proj,
    gate_proj,
    out_proj,
    value_scale,
    gate_scale,
    out_scale,
    conv_kernel,
    norm_gain,
    norm_shift,
    mlp_gain,
    mlp_gate,
    mlp_up,
    mlp_down,
    mlp_gate_scale,
    mlp_up_scale,
    mlp_down_scale,
):
    out_full, down_full = (
        lax.all_gather(out_scale, "fs", axis=0, tiled=True),
        lax.all_gather(mlp_down_scale, "fs", axis=0, tiled=True),
    )
    value_w, gate_w, out_w = (
        lax.all_gather(value_proj.astype(jnp.bfloat16), "fs", axis=0, tiled=True),
        lax.all_gather(gate_proj.astype(jnp.bfloat16), "fs", axis=0, tiled=True),
        lax.all_gather(out_proj.astype(jnp.bfloat16), "fs", axis=0, tiled=True),
    )
    mlp_shards = (
        mlp_gate.astype(jnp.bfloat16),
        mlp_up.astype(jnp.bfloat16),
        mlp_down.astype(jnp.bfloat16),
    )
    rows = hidden_in.astype(jnp.float32)
    normed = row_norm(rows, mix_gain).astype(jnp.bfloat16)
    value_pre = jnp.dot(normed, value_w, preferred_element_type=jnp.float32) * value_scale
    gate_pre = jnp.dot(normed, gate_w, preferred_element_type=jnp.float32) * gate_scale
    glu = value_pre * jax.nn.sigmoid(gate_pre)
    seq_len = glu.shape[0]
    taps = conv_kernel.shape[0]
    padded = jnp.pad(glu, ((taps - 1, 0), (0, 0)))
    kernel = conv_kernel.astype(jnp.float32)
    conved = jnp.zeros_like(glu)
    for tap in range(taps):
        conved = conved + padded[tap : tap + seq_len] * kernel[tap]
    channels = conved.shape[1] * lax.axis_size("tp")
    sums, squares = lax.psum((jnp.sum(conved, axis=1), jnp.sum(conved * conved, axis=1)), "tp")
    chan_mean = (sums / channels)[:, None]
    chan_var = (squares / channels)[:, None] - chan_mean * chan_mean
    act = jax.nn.silu(
        (conved - chan_mean) * lax.rsqrt(chan_var + 1e-05) * norm_gain + norm_shift
    ).astype(jnp.bfloat16)
    conv_term = contract_last(act, out_w) * out_full
    middle_f = (
        (rows + lax.psum(conv_term.astype(jnp.bfloat16), "tp").astype(jnp.float32))
        .astype(jnp.bfloat16)
        .astype(jnp.float32)
    )
    normed_mlp = row_norm(middle_f, mlp_gain).astype(jnp.bfloat16)
    collected = (
        lax.all_gather(mlp_shards[0], "fs", axis=0, tiled=True),
        lax.all_gather(mlp_shards[1], "fs", axis=0, tiled=True),
        lax.all_gather(mlp_shards[2], "fs", axis=0, tiled=True),
    )
    gate_mlp = (
        jnp.dot(normed_mlp, collected[0], preferred_element_type=jnp.float32) * mlp_gate_scale
    )
    up_mlp = jnp.dot(normed_mlp, collected[1], preferred_element_type=jnp.float32) * mlp_up_scale
    hidden_act = (jax.nn.silu(gate_mlp) * up_mlp).astype(jnp.bfloat16)
    mlp_term = contract_last(hidden_act, collected[2]) * down_full
    return (middle_f + lax.psum(mlp_term.astype(jnp.bfloat16), "tp").astype(jnp.float32)).astype(
        jnp.bfloat16
    )


def solution(mesh):
    return jax.shard_map(
        body,
        mesh=mesh,
        in_specs=(
            P("fs", None),
            P(),
            P("fs", "tp"),
            P("fs", "tp"),
            P("fs", "tp"),
            P("tp"),
            P("tp"),
            P("fs"),
            P(None, "tp"),
            P("tp"),
            P("tp"),
            P(),
            P("fs", "tp"),
            P("fs", "tp"),
            P("fs", "tp"),
            P("tp"),
            P("tp"),
            P("fs"),
        ),
        out_specs=P("fs", None),
        check_vma=False,
    )
```

profile of v0, /device:TPU:0, one launch (start us, length us, event | category | flops | bytes accessed | tf_op | source)
XLA Modules:
  0.0 370.3 jit_solution(7887861853661166801)
XLA Ops:
  7.4 0.0 all-reduce.5.cloned.1.call-start
  7.4 0.8 convert_element_type.63
  8.2 1.5 fusion.2
  9.8 0.9 convert_element_type.61
  10.7 33.0 %all_gather.24 = bf16[2048,128]{1,0:T(8,128)(2,1)S(1)} all-gather(bf16[256,128]{1,0:T(8,128)(2,1)S(1)} %convert_element_type.61), channel_id=1, replica_groups=mesh['fs'=8,'tp'=4] {'fs'}, dimensions={0}, use_global_device_ids=true | all-gather | bytes 589824 | tf_op jit(solution)/shard_map/all_gather | solution.py:43
  43.7 0.9 convert_element_type.62
  44.6 31.4 %all_gather.25 = bf16[2048,128]{1,0:T(8,128)(2,1)S(1)} all-gather(bf16[256,128]{1,0:T(8,128)(2,1)S(1)} %convert_element_type.62), channel_id=1, replica_groups=mesh['fs'=8,'tp'=4] {'fs'}, dimensions={0}, use_global_device_ids=true | all-gather | bytes 589824 | tf_op jit(solution)/shard_map/all_gather | solution.py:44
  76.0 0.0 copy-done.4
  76.0 31.3 %all_gather.26 = bf16[2048,128]{1,0:T(8,128)(2,1)S(1)} all-gather(bf16[256,128]{1,0:T(8,128)(2,1)S(1)} %convert_element_type.65), channel_id=1, replica_groups=mesh['fs'=8,'tp'=4] {'fs'}, dimensions={0}, use_global_device_ids=true | all-gather | bytes 589824 | tf_op jit(solution)/shard_map/all_gather | solution.py:45
  107.3 20.7 %all-gather = f32[8,1,256]{2,1,0:T(1,128)S(1)} all-gather(f32[1,1,256]{2,1,0:T(1,128)S(1)} %bitcast.74), channel_id=1, replica_groups=mesh['fs'=8,'tp'=4] {'fs'}, dimensions={0}, use_global_device_ids=true | all-gather | bytes 9216 | tf_op jit(solution)/shard_map/all_gather | solution.py:39
  128.1 0.0 copy-done
  128.1 0.0 copy-done.11
  128.1 0.5 convolution_multiply_fusion.5
  128.6 0.0 copy-start.13
  128.6 0.0 copy-start.14
  128.6 0.5 fusion.16
  129.1 0.0 copy-start.1
  129.2 0.6 fusion.91
  129.7 5.7 %all-reduce.1 = (f32[256]{0:T(256)S(1)}, f32[256]{0:T(256)S(1)}) all-reduce(f32[256]{0:T(256)S(1)} %get-tuple-element.6, f32[256]{0:T(256)S(1)} %get-tuple-element.5), channel_id=1, replica_groups=mesh['fs'=8,'tp'=4] {'tp'}, use_global_device_ids=true, to_apply=%region_4.5 | all-reduce | flops 512 | bytes 4096 | tf_op jit(solution)/shard_map/psum | solution.py:65
  135.4 0.0 copy-start.2
  135.4 1.5 fusion.1
  136.9 0.0 all-reduce.5.cloned.1.call-update
  136.9 0.0 copy-start.6
  136.9 0.0 all-gather.6.cloned.1.call-start
  137.0 0.8 convert_element_type.71
  137.8 0.0 all-gather.6.cloned.1.call-update
  137.8 0.0 all-gather.10.cloned.1.call-start
  137.9 0.0 copy-done.2
  137.9 0.8 convert_element_type.74
  138.6 0.0 all-gather.10.cloned.1.call-update
  138.7 0.0 copy-start.8
  138.7 0.0 copy-start.9
  138.7 0.0 all-gather.8.cloned.1.call-start
  138.7 0.0 copy-done.3
  138.8 0.8 convert_element_type.72
  139.6 0.0 all-gather.8.cloned.1.call-update
  139.6 0.0 all-reduce.7.cloned.1.call-start
  139.6 16.5 %all-gather.1 = f32[8,1,256]{2,1,0:T(1,128)S(1)} all-gather(f32[1,1,256]{2,1,0:T(1,128)S(1)} %bitcast.75), channel_id=1, replica_groups=mesh['fs'=8,'tp'=4] {'fs'}, dimensions={0}, use_global_device_ids=true | all-gather | bytes 9216 | tf_op jit(solution)/shard_map/all_gather | solution.py:40
  156.2 14.7 %all-reduce.5.cloned.1.call-done = bf16[256,2048]{1,0:T(8,128)(2,1)} async-done(((bf16[256,2048]{1,0:T(8,128)(2,1)}), bf16[256,2048]{1,0:T(8,128)(2,1)}) %all-reduce.5.cloned.1.call-update) | async-done | bytes 1048592 | tf_op jit(solution)/shard_map/psum | solution.py:73
  170.9 1.8 fusion.6
  172.6 24.8 %all-gather.6.cloned.1.call-done = bf16[2048,704]{0,1:T(8,128)(2,1)} async-done(((bf16[256,704]{0,1:T(8,128)(2,1)}), bf16[2048,704]{0,1:T(8,128)(2,1)}) %all-gather.6.cloned.1.call-update) | async-done | bytes 2883600 | tf_op jit(solution)/shard_map/all_gather | solution.py:79
  197.4 2.8 convolution_multiply_fusion.3
  200.3 57.6 %all-gather.10.cloned.1.call-done = bf16[2048,704]{0,1:T(8,128)(2,1)} async-done(((bf16[256,704]{0,1:T(8,128)(2,1)}), bf16[2048,704]{0,1:T(8,128)(2,1)}) %all-gather.10.cloned.1.call-update) | async-done | bytes 2883600 | tf_op jit(solution)/shard_map/all_gather | solution.py:81
  257.9 60.5 %all-gather.8.cloned.1.call-done = bf16[2048,704]{0,1:T(8,128)(2,1)} async-done(((bf16[256,704]{0,1:T(8,128)(2,1)}), bf16[2048,704]{0,1:T(8,128)(2,1)}) %all-gather.8.cloned.1.call-update) | async-done | bytes 2883600 | tf_op jit(solution)/shard_map/all_gather | solution.py:80
  318.5 7.0 %fusion = bf16[256,2048]{1,0:T(8,128)(2,1)} fusion(bf16[2048,704]{0,1:T(8,128)(2,1)} %all-gather.10.cloned.1.call-done, f32[2048]{0:T(1024)S(1)} %bitcast.73, bf16[2048,704]{0,1:T(8,128)(2,1)} %all-gather.8.cloned.1.call-done, f32[256,704]{0,1:T(8,128)S(1)} %convolution_multiply_fusion.3, f32[704]{0:T(1024)S(1)} %copy-done.10, ...), kind=kOutput, calls=%fused_computation.8 | convolution fusion | flops 1480802304 | bytes 8605440 | tf_op jit(solution)/shard_map/dot_general | solution.py:13
  325.5 0.0 all-reduce.7.cloned.1.call-update
  325.5 34.6 %all-reduce.7.cloned.1.call-done = bf16[256,2048]{1,0:T(8,128)(2,1)} async-done(((bf16[256,2048]{1,0:T(8,128)(2,1)}), bf16[256,2048]{1,0:T(8,128)(2,1)}) %all-reduce.7.cloned.1.call-update) | async-done | bytes 1048592 | tf_op jit(solution)/shard_map/psum | solution.py:89
  360.1 2.6 fusion.9
  (24 shorter events, 0.1 us)
Async XLA Ops:
  7.4 120.7 %copy-start = (bf16[256,2048]{1,0:T(8,128)(2,1)S(1)}, bf16[256,2048]{1,0:T(8,128)(2,1)}, u32[]{:S(2)}) copy-start(bf16[256,2048]{1,0:T(8,128)(2,1)} %param.18) | copy-start | bytes 3145732
  7.4 68.6 %copy-start.4 = (f32[256,128]{1,0:T(8,128)S(1)}, f32[256,128]{1,0:T(8,128)}, u32[]{:S(2)}) copy-start(f32[256,128]{1,0:T(8,128)} %param.22) | copy-start | bytes 393220
  7.4 100.0 %copy-start.5 = (f32[256]{0:T(256)S(1)}, f32[256]{0:T(256)}, u32[]{:S(2)}) copy-start(f32[256]{0:T(256)} %param.25) | copy-start | bytes 3076
  7.4 120.7 %copy-start.7 = (f32[2048]{0:T(1024)S(1)}, f32[2048]{0:T(1024)}, u32[]{:S(2)}) copy-start(f32[2048]{0:T(1024)} %param.19) | copy-start | bytes 24580
  7.4 120.7 %copy-start.11 = (f32[128]{0:T(128)S(1)}, f32[128]{0:T(128)}, u32[]{:S(2)}) copy-start(f32[128]{0:T(128)} %param.23) | copy-start | bytes 1540
  7.4 163.5 %all-reduce.5.cloned.1.call-start = ((), (), s32[]{:S(2)}) async-start(), calls=%async_computation | async-start | bytes 2097152 | tf_op jit(solution)/shard_map/psum | solution.py:73
  43.7 84.9 %copy-start.12 = (f32[128]{0:T(128)S(1)}, f32[128]{0:T(128)}, u32[]{:S(2)}) copy-start(f32[128]{0:T(128)} %param.24) | copy-start | bytes 1540
  128.6 6.8 %copy-start.13 = (f32[128]{0:T(128)S(1)}, f32[128]{0:T(128)}, u32[]{:S(2)}) copy-start(f32[128]{0:T(128)} %param.28) | copy-start | bytes 1540
  128.6 6.8 %copy-start.14 = (f32[128]{0:T(128)S(1)}, f32[128]{0:T(128)}, u32[]{:S(2)}) copy-start(f32[128]{0:T(128)} %param.27) | copy-start | bytes 1540
  129.1 7.9 %copy-start.1 = (f32[256,704]{0,1:T(8,128)S(1)}, f32[256,704]{0,1:T(8,128)}, u32[]{:S(2)}) copy-start(f32[256,704]{0,1:T(8,128)} %param.30) | copy-start | bytes 2162692
  135.4 2.5 copy-start.2
  136.9 1.8 copy-start.3
  136.9 2.7 copy-start.6
  136.9 60.5 %all-gather.6.cloned.1.call-start = ((), (), s32[]{:S(2)}) async-start(), calls=%async_computation.1 | async-start | bytes 3244032 | tf_op jit(solution)/shard_map/all_gather | solution.py:79
  137.8 120.1 %all-gather.10.cloned.1.call-start = ((), (), s32[]{:S(2)}) async-start(), calls=%async_computation.3 | async-start | bytes 3244032 | tf_op jit(solution)/shard_map/all_gather | solution.py:81
  138.7 58.8 %copy-start.8 = (f32[2048]{0:T(1024)S(1)}, f32[2048]{0:T(1024)}, u32[]{:S(2)}) copy-start(f32[2048]{0:T(1024)} %param.29) | copy-start | bytes 24580
  138.7 58.8 %copy-start.9 = (f32[704]{0:T(1024)S(1)}, f32[704]{0:T(1024)}, u32[]{:S(2)}) copy-start(f32[704]{0:T(1024)} %param.33) | copy-start | bytes 8452
  138.7 179.8 %all-gather.8.cloned.1.call-start = ((), (), s32[]{:S(2)}) async-start(), calls=%async_computation.2 | async-start | bytes 3244032 | tf_op jit(solution)/shard_map/all_gather | solution.py:80
  139.6 220.6 %all-reduce.7.cloned.1.call-start = ((), (), s32[]{:S(2)}) async-start(), calls=%async_computation.4 | async-start | bytes 2097152 | tf_op jit(solution)/shard_map/psum | solution.py:89
  197.4 121.0 %copy-start.10 = (f32[704]{0:T(1024)S(1)}, f32[704]{0:T(1024)}, u32[]{:S(2)}) copy-start(f32[704]{0:T(1024)} %param.34) | copy-start | bytes 8452
Sparse Core Ops, SparseCore 0:
  137.1 33.7 all-reduce.4
  325.6 34.4 all-reduce.6
Sparse Core Ops, SparseCore 1:
  139.5 57.9 all-gather.5
  199.3 58.5 all-gather.9
  259.9 58.5 all-gather.7
where the time goes:
time: 371 us; the launch traced here: 370 us
  waiting for transfers between devices  192 us (52%)
  blocking collectives  139 us (37%)
  between operations  15.2 us (4%)
  matrix products  12.4 us (3%)
  other arithmetic  11.4 us (3%)
    all_gather x1, waiting for transfers between devices, body(): lax.all_gather(mlp_shards[1], 'fs', axis=0, tiled=True)  60.5 us
    all_gather x1, waiting for transfers between devices, body(): lax.all_gather(mlp_shards[2], 'fs', axis=0, tiled=True)  57.6 us
    psum x1, waiting for transfers between devices, body(): lax.psum(mlp_term.astype(jnp.bfloat16), 'tp').astype(jnp.float32)  34.6 us
    all_gather x1, blocking collectives, body(): lax.all_gather(value_proj.astype(jnp.bfloat16), 'fs', axis=0, tiled=True)  33 us
    all_gather x1, blocking collectives, body(): lax.all_gather(gate_proj.astype(jnp.bfloat16), 'fs', axis=0, tiled=True)  31.4 us
    all_gather x1, blocking collectives, body(): lax.all_gather(out_proj.astype(jnp.bfloat16), 'fs', axis=0, tiled=True)  31.3 us
    all_gather x1, waiting for transfers between devices, body(): lax.all_gather(mlp_shards[0], 'fs', axis=0, tiled=True)  24.8 us
    all_gather x1, blocking collectives, body(): lax.all_gather(out_scale, 'fs', axis=0, tiled=True)  20.7 us
  transfers between devices with their start and end apart: 5, of which 5 were waited for; matrix products, arithmetic and copies ran while one was open for 2% of the time, Pallas kernels for 0%

commit v1 on v0

--- a/solution.py
+++ b/solution.py
@@ -2,6 +2,22 @@
 import jax.numpy as jnp
 from jax import lax
 from jax.sharding import PartitionSpec as P
+
+
+def collect(x, axis, dim):
+    ways, here, lap = (lax.axis_size(axis), lax.axis_index(axis), x.shape[dim])
+    shape = [n * ways if d == dim else n for d, n in enumerate(x.shape)]
+    full = lax.dynamic_update_slice_in_dim(jnp.zeros(shape, x.dtype), x, here * lap, axis=dim)
+    going_up = going_down = x
+    for far in range(1, ways // 2 + 1):
+        going_up = lax.ppermute(going_up, axis, [(d, (d + 1) % ways) for d in range(ways)])
+        full = lax.dynamic_update_slice_in_dim(full, going_up, (here - far) % ways * lap, axis=dim)
+        if 2 * far < ways:
+            going_down = lax.ppermute(going_down, axis, [(d, (d - 1) % ways) for d in range(ways)])
+            full = lax.dynamic_update_slice_in_dim(
+                full, going_down, (here + far) % ways * lap, axis=dim
+            )
+    return full
 
 
 def row_norm(rows, gain):
@@ -77,7 +93,7 @@
     normed_mlp = row_norm(middle_f, mlp_gain).astype(jnp.bfloat16)
     collected = (
         lax.all_gather(mlp_shards[0], "fs", axis=0, tiled=True),
-        lax.all_gather(mlp_shards[1], "fs", axis=0, tiled=True),
+        collect(mlp_shards[1], "fs", 0),
         lax.all_gather(mlp_shards[2], "fs", axis=0, tiled=True),
     )
     gate_mlp = (

time: 371 us -> 349 us (0.941)
  waiting for transfers between devices: 192 us -> 139 us
  starting transfers between devices: 0.21 us -> 14.4 us
  blocking collectives: 139 us -> 148 us
  local copies, waits for them, and re-layouts: 0.09 us -> 7.63 us
    all_gather x1 -> x0, waiting for transfers between devices: 60.5 us -> none  [body(): lax.all_gather(mlp_shards[1], 'fs', axis=0, tiled=True)]
    ppermute x0 -> x7, waiting for transfers between devices: none -> 45.2 us  [the longest x3 26.2 us: collect(): lax.ppermute(going_down, axis, [(d, (d - 1) % ways) for d in range(ways)])]
    all_gather x1, waiting for transfers between devices: 24.8 us -> 0.01 us  [body(): lax.all_gather(mlp_shards[0], 'fs', axis=0, tiled=True)]
    psum x1, waiting for transfers between devices: 14.7 us -> 0.01 us  [body(): lax.psum(conv_term.astype(jnp.bfloat16), 'tp').astype(jnp.float32)]
    ppermute x0 -> x7, starting transfers between devices: none -> 14.2 us  [the longest x4 7.14 us: collect(): lax.ppermute(going_up, axis, [(d, (d + 1) % ways) for d in range(ways)])]
    all_gather x1, blocking collectives: 16.5 us -> 25.7 us  [body(): lax.all_gather(mlp_down_scale, 'fs', axis=0, tiled=True)]
    dynamic_update_slice x0 -> x7, local copies, waits for them, and re-layouts: none -> 5.56 us  [the longest x4 3.18 us: collect(): lax.dynamic_update_slice_in_dim(full, going_up, (here - far) % ways * lap...]
  transfers between devices with their start and end apart: 5 -> 11, of which waited for: 5 -> 6; matrix products, arithmetic and copies ran while one was open for 2% -> 4% of each run, Pallas kernels for 0% -> 0%
where the time goes in v1:
time: 349 us
  blocking collectives  148 us (42%)
  waiting for transfers between devices  139 us (40%)
  between operations  15 us (4%)
  starting transfers between devices  14.4 us (4%)
  matrix products  12.5 us (4%)
  other arithmetic  12.4 us (4%)
  local copies, waits for them, and re-layouts  7.63 us (2%)
    all_gather x1, waiting for transfers between devices, body(): lax.all_gather(mlp_shards[2], 'fs', axis=0, tiled=True)  59.5 us
    psum x1, waiting for transfers between devices, body(): lax.psum(mlp_term.astype(jnp.bfloat16), 'tp').astype(jnp.float32)  34.6 us
    all_gather x1, blocking collectives, body(): lax.all_gather(value_proj.astype(jnp.bfloat16), 'fs', axis=0, tiled=True)  33 us
    all_gather x1, blocking collectives, body(): lax.all_gather(gate_proj.astype(jnp.bfloat16), 'fs', axis=0, tiled=True)  31.4 us
    all_gather x1, blocking collectives, body(): lax.all_gather(out_proj.astype(jnp.bfloat16), 'fs', axis=0, tiled=True)  31.4 us
    ppermute x3, waiting for transfers between devices, collect(): lax.ppermute(going_down, axis, [(d, (d - 1) % ways) for d in range(ways)])  26.2 us
    all_gather x1, blocking collectives, body(): lax.all_gather(mlp_down_scale, 'fs', axis=0, tiled=True)  25.7 us
    all_gather x1, blocking collectives, body(): lax.all_gather(out_scale, 'fs', axis=0, tiled=True)  20.6 us
  transfers between devices with their start and end apart: 11, of which 6 were waited for; matrix products, arithmetic and copies ran while one was open for 4% of the time, Pallas kernels for 0%

profile of v1, /device:TPU:0, one launch (start us, length us, event | category | flops | bytes accessed | tf_op | source)
XLA Modules:
  0.0 349.0 jit_solution(7002372015008516786)
XLA Ops:
  7.4 0.0 all-reduce.5.cloned.1.call-start
  7.4 0.8 convert_element_type.63
  8.2 1.5 fusion.2
  9.8 0.9 convert_element_type.61
  10.7 33.0 %all_gather.21 = bf16[2048,128]{1,0:T(8,128)(2,1)S(1)} all-gather(bf16[256,128]{1,0:T(8,128)(2,1)S(1)} %convert_element_type.61), channel_id=1, replica_groups=mesh['fs'=8,'tp'=4] {'fs'}, dimensions={0}, use_global_device_ids=true | all-gather | bytes 589824 | tf_op jit(solution)/shard_map/all_gather | solution.py:59
  43.7 0.9 convert_element_type.62
  44.6 31.4 %all_gather.22 = bf16[2048,128]{1,0:T(8,128)(2,1)S(1)} all-gather(bf16[256,128]{1,0:T(8,128)(2,1)S(1)} %convert_element_type.62), channel_id=1, replica_groups=mesh['fs'=8,'tp'=4] {'fs'}, dimensions={0}, use_global_device_ids=true | all-gather | bytes 589824 | tf_op jit(solution)/shard_map/all_gather | solution.py:60
  76.0 0.9 convert_element_type.65
  76.9 31.4 %all_gather.23 = bf16[2048,128]{1,0:T(8,128)(2,1)S(1)} all-gather(bf16[256,128]{1,0:T(8,128)(2,1)S(1)} %convert_element_type.65), channel_id=1, replica_groups=mesh['fs'=8,'tp'=4] {'fs'}, dimensions={0}, use_global_device_ids=true | all-gather | bytes 589824 | tf_op jit(solution)/shard_map/all_gather | solution.py:61
  108.3 20.6 %all-gather = f32[8,1,256]{2,1,0:T(1,128)S(1)} all-gather(f32[1,1,256]{2,1,0:T(1,128)S(1)} %bitcast.74), channel_id=1, replica_groups=mesh['fs'=8,'tp'=4] {'fs'}, dimensions={0}, use_global_device_ids=true | all-gather | bytes 9216 | tf_op jit(solution)/shard_map/all_gather | solution.py:55
  128.9 0.5 convolution_multiply_fusion.5
  129.4 0.5 fusion.16
  130.0 0.6 fusion.91
  130.5 5.7 %all-reduce.1 = (f32[256]{0:T(256)S(1)}, f32[256]{0:T(256)S(1)}) all-reduce(f32[256]{0:T(256)S(1)} %get-tuple-element.6, f32[256]{0:T(256)S(1)} %get-tuple-element.5), channel_id=1, replica_groups=mesh['fs'=8,'tp'=4] {'tp'}, use_global_device_ids=true, to_apply=%region_4.5 | all-reduce | flops 512 | bytes 4096 | tf_op jit(solution)/shard_map/psum | solution.py:81
  136.2 1.5 fusion.1
  137.7 0.0 all-gather.5.cloned.1.call-start
  137.8 0.8 convert_element_type.71
  138.6 0.0 all-gather.5.cloned.1.call-update
  138.6 0.0 all-gather.7.cloned.1.call-start
  138.7 0.8 convert_element_type.74
  139.5 0.0 all-gather.7.cloned.1.call-update
  139.5 0.0 all-reduce.7.cloned.1.call-start
  139.5 2.0 broadcast_in_dim.2
  141.5 0.8 constant_dynamic-update-slice_fusion.7
  142.4 4.7 %collective-permute-start.1 = (bf16[256,704]{0,1:T(8,128)(2,1)S(1)}, bf16[256,704]{0,1:T(8,128)(2,1)S(1)}, u32[]{:S(2)}, u32[]{:S(2)}) collective-permute-start(bf16[256,704]{0,1:T(8,128)(2,1)S(1)} %get-tuple-element.12), channel_id=1, source_target_pairs={{0,28},{4,0},{8,4},{12,8},{16,12},{20,16},{24,20},{28,24},{1,29},{... | collective-permute-start | bytes 1081352 | tf_op jit(solution)/shard_map/ppermute | solution.py:16
  147.1 14.8 %collective-permute-done = bf16[256,704]{0,1:T(8,128)(2,1)S(1)} collective-permute-done((bf16[256,704]{0,1:T(8,128)(2,1)S(1)}, bf16[256,704]{0,1:T(8,128)(2,1)S(1)}, u32[]{:S(2)}, u32[]{:S(2)}) %collective-permute-start) | collective-permute-done | bytes 360480 | tf_op jit(solution)/shard_map/ppermute | solution.py:13
  161.9 2.5 collective-permute-start.2
  164.4 25.7 %all-gather.1 = f32[8,1,256]{2,1,0:T(1,128)S(1)} all-gather(f32[1,1,256]{2,1,0:T(1,128)S(1)} %bitcast.75), channel_id=1, replica_groups=mesh['fs'=8,'tp'=4] {'fs'}, dimensions={0}, use_global_device_ids=true | all-gather | bytes 9216 | tf_op jit(solution)/shard_map/all_gather | solution.py:56
  190.1 2.4 collective-permute-start.3
  192.5 0.8 constant_dynamic-update-slice_fusion.6
  193.3 0.8 constant_dynamic-update-slice_fusion.5
  194.1 0.0 collective-permute-start.4
  194.1 1.7 fusion.6
  195.9 20.0 %collective-permute-done.3 = bf16[256,704]{0,1:T(8,128)(2,1)S(1)} collective-permute-done((bf16[256,704]{0,1:T(8,128)(2,1)S(1)}, bf16[256,704]{0,1:T(8,128)(2,1)S(1)}, u32[]{:S(2)}, u32[]{:S(2)}) %collective-permute-start.3) | collective-permute-done | bytes 360480 | tf_op jit(solution)/shard_map/ppermute | solution.py:16
  215.9 0.8 constant_dynamic-update-slice_fusion.4
  216.7 4.6 %collective-permute-start.6 = (bf16[256,704]{0,1:T(8,128)(2,1)S(1)}, bf16[256,704]{0,1:T(8,128)(2,1)S(1)}, u32[]{:S(2)}, u32[]{:S(2)}) collective-permute-start(bf16[256,704]{0,1:T(8,128)(2,1)S(1)} %collective-permute-done.4), channel_id=1, source_target_pairs={{0,4},{4,8},{8,12},{12,16},{16,20},{20,24},{24,28},{28,0},{1,5},{5... | collective-permute-start | bytes 1081352 | tf_op jit(solution)/shard_map/ppermute | solution.py:13
  221.3 0.8 constant_dynamic-update-slice_fusion.3
  222.1 0.8 constant_dynamic-update-slice_fusion.2
  222.8 6.2 %collective-permute-done.5 = bf16[256,704]{0,1:T(8,128)(2,1)S(1)} collective-permute-done((bf16[256,704]{0,1:T(8,128)(2,1)S(1)}, bf16[256,704]{0,1:T(8,128)(2,1)S(1)}, u32[]{:S(2)}, u32[]{:S(2)}) %collective-permute-start.5) | collective-permute-done | bytes 360480 | tf_op jit(solution)/shard_map/ppermute | solution.py:16
  229.0 0.8 constant_dynamic-update-slice_fusion.1
  229.9 4.2 %collective-permute-done.6 = bf16[256,704]{0,1:T(8,128)(2,1)S(1)} collective-permute-done((bf16[256,704]{0,1:T(8,128)(2,1)S(1)}, bf16[256,704]{0,1:T(8,128)(2,1)S(1)}, u32[]{:S(2)}, u32[]{:S(2)}) %collective-permute-start.6) | collective-permute-done | bytes 360480 | tf_op jit(solution)/shard_map/ppermute | solution.py:13
  234.1 0.8 constant_dynamic-update-slice_fusion
  234.9 2.9 convolution_multiply_fusion.3
  237.8 59.5 %all-gather.7.cloned.1.call-done = bf16[2048,704]{0,1:T(8,128)(2,1)} async-done(((bf16[256,704]{0,1:T(8,128)(2,1)}), bf16[2048,704]{0,1:T(8,128)(2,1)}) %all-gather.7.cloned.1.call-update) | async-done | bytes 2883600 | tf_op jit(solution)/shard_map/all_gather | solution.py:97
  297.3 7.0 %fusion = bf16[256,2048]{1,0:T(8,128)(2,1)} fusion(bf16[2048,704]{0,1:T(8,128)(2,1)} %all-gather.7.cloned.1.call-done, f32[2048]{0:T(1024)S(1)} %bitcast.72, bf16[2048,704]{0,1:T(8,128)(2,1)} %constant_dynamic-update-slice_fusion, f32[256,704]{0,1:T(8,128)S(1)} %convolution_multiply_fusion.3, f32[704]{0:T(1024)S(1)} %copy-done.9, ...), kind=kOutput, calls=%fused_computation.8 | convolution fusion | flops 1480802304 | bytes 8605440 | tf_op jit(solution)/shard_map/dot_general | solution.py:29
  304.4 0.0 all-reduce.7.cloned.1.call-update
  304.4 34.6 %all-reduce.7.cloned.1.call-done = bf16[256,2048]{1,0:T(8,128)(2,1)} async-done(((bf16[256,2048]{1,0:T(8,128)(2,1)}), bf16[256,2048]{1,0:T(8,128)(2,1)}) %all-reduce.7.cloned.1.call-update) | async-done | bytes 1048592 | tf_op jit(solution)/shard_map/psum | solution.py:105
  339.0 2.6 fusion.9
  (41 shorter events, 0.1 us)
Async XLA Ops:
  7.4 121.5 %copy-start = (bf16[256,2048]{1,0:T(8,128)(2,1)S(1)}, bf16[256,2048]{1,0:T(8,128)(2,1)}, u32[]{:S(2)}) copy-start(bf16[256,2048]{1,0:T(8,128)(2,1)} %param.18) | copy-start | bytes 3145732
  7.4 100.9 %copy-start.4 = (f32[256]{0:T(256)S(1)}, f32[256]{0:T(256)}, u32[]{:S(2)}) copy-start(f32[256]{0:T(256)} %param.25) | copy-start | bytes 3076
  7.4 121.5 %copy-start.6 = (f32[2048]{0:T(1024)S(1)}, f32[2048]{0:T(1024)}, u32[]{:S(2)}) copy-start(f32[2048]{0:T(1024)} %param.19) | copy-start | bytes 24580
  7.4 121.5 %copy-start.10 = (f32[128]{0:T(128)S(1)}, f32[128]{0:T(128)}, u32[]{:S(2)}) copy-start(f32[128]{0:T(128)} %param.23) | copy-start | bytes 1540
  7.4 186.8 %all-reduce.5.cloned.1.call-start = ((), (), s32[]{:S(2)}) async-start(), calls=%async_computation | async-start | bytes 2097152 | tf_op jit(solution)/shard_map/psum | solution.py:89
  8.2 121.2 %copy-start.11 = (f32[128]{0:T(128)S(1)}, f32[128]{0:T(128)}, u32[]{:S(2)}) copy-start(f32[128]{0:T(128)} %param.24) | copy-start | bytes 1540
  128.9 7.3 %copy-start.12 = (f32[128]{0:T(128)S(1)}, f32[128]{0:T(128)}, u32[]{:S(2)}) copy-start(f32[128]{0:T(128)} %param.28) | copy-start | bytes 1540
  128.9 7.3 %copy-start.13 = (f32[128]{0:T(128)S(1)}, f32[128]{0:T(128)}, u32[]{:S(2)}) copy-start(f32[128]{0:T(128)} %param.27) | copy-start | bytes 1540
  129.4 8.4 %copy-start.1 = (f32[256,704]{0,1:T(8,128)S(1)}, f32[256,704]{0,1:T(8,128)}, u32[]{:S(2)}) copy-start(f32[256,704]{0,1:T(8,128)} %param.30) | copy-start | bytes 2162692
  130.0 8.7 %copy-start.2 = (f32[256,704]{0,1:T(8,128)S(1)}, f32[256,704]{0,1:T(8,128)}, u32[]{:S(2)}) copy-start(f32[256,704]{0,1:T(8,128)} %param.32) | copy-start | bytes 2162692
  137.7 3.8 %copy-start.3 = (f32[256,704]{0,1:T(8,128)S(1)}, f32[256,704]{0,1:T(8,128)}, u32[]{:S(2)}) copy-start(f32[256,704]{0,1:T(8,128)} %param.31) | copy-start | bytes 2162692
  137.7 97.1 %all-gather.5.cloned.1.call-start = ((), (), s32[]{:S(2)}) async-start(), calls=%async_computation.1 | async-start | bytes 3244032 | tf_op jit(solution)/shard_map/all_gather | solution.py:95
  138.6 25.8 %copy-start.5 = (f32[256]{0:T(256)S(1)}, f32[256]{0:T(256)}, u32[]{:S(2)}) copy-start(f32[256]{0:T(256)} %param.35) | copy-start | bytes 3076
  138.6 158.7 %all-gather.7.cloned.1.call-start = ((), (), s32[]{:S(2)}) async-start(), calls=%async_computation.2 | async-start | bytes 3244032 | tf_op jit(solution)/shard_map/all_gather | solution.py:97
  139.5 199.5 %all-reduce.7.cloned.1.call-start = ((), (), s32[]{:S(2)}) async-start(), calls=%async_computation.3 | async-start | bytes 2097152 | tf_op jit(solution)/shard_map/psum | solution.py:105
  142.4 19.6 %collective-permute-start = (bf16[256,704]{0,1:T(8,128)(2,1)S(1)}, bf16[256,704]{0,1:T(8,128)(2,1)S(1)}, u32[]{:S(2)}, u32[]{:S(2)}) collective-permute-start(bf16[256,704]{0,1:T(8,128)(2,1)S(1)} %get-tuple-element.12), channel_id=1, source_target_pairs={{0,4},{4,8},{8,12},{12,16},{16,20},{20,24},{24,28},{28,0},{1,5},{5... | collective-permute-start | bytes 1081352 | tf_op jit(solution)/shard_map/ppermute | solution.py:13
  142.4 47.8 %collective-permute-start.1 = (bf16[256,704]{0,1:T(8,128)(2,1)S(1)}, bf16[256,704]{0,1:T(8,128)(2,1)S(1)}, u32[]{:S(2)}, u32[]{:S(2)}) collective-permute-start(bf16[256,704]{0,1:T(8,128)(2,1)S(1)} %get-tuple-element.12), channel_id=1, source_target_pairs={{0,28},{4,0},{8,4},{12,8},{16,12},{20,16},{24,20},{28,24},{1,29},{... | collective-permute-start | bytes 1081352 | tf_op jit(solution)/shard_map/ppermute | solution.py:16
  161.9 32.2 %collective-permute-start.2 = (bf16[256,704]{0,1:T(8,128)(2,1)S(1)}, bf16[256,704]{0,1:T(8,128)(2,1)S(1)}, u32[]{:S(2)}, u32[]{:S(2)}) collective-permute-start(bf16[256,704]{0,1:T(8,128)(2,1)S(1)} %collective-permute-done), channel_id=1, source_target_pairs={{0,4},{4,8},{8,12},{12,16},{16,20},{20,24},{24,28},{28,0},{1,5},{5... | collective-permute-start | bytes 1081352 | tf_op jit(solution)/shard_map/ppermute | solution.py:13
  190.1 25.7 %collective-permute-start.3 = (bf16[256,704]{0,1:T(8,128)(2,1)S(1)}, bf16[256,704]{0,1:T(8,128)(2,1)S(1)}, u32[]{:S(2)}, u32[]{:S(2)}) collective-permute-start(bf16[256,704]{0,1:T(8,128)(2,1)S(1)} %collective-permute-done.1), channel_id=1, source_target_pairs={{0,28},{4,0},{8,4},{12,8},{16,12},{20,16},{24,20},{28,24},{1,29},{... | collective-permute-start | bytes 1081352 | tf_op jit(solution)/shard_map/ppermute | solution.py:16
  194.1 40.8 %copy-start.8 = (f32[704]{0:T(1024)S(1)}, f32[704]{0:T(1024)}, u32[]{:S(2)}) copy-start(f32[704]{0:T(1024)} %param.33) | copy-start | bytes 8452
  194.1 22.6 %collective-permute-start.4 = (bf16[256,704]{0,1:T(8,128)(2,1)S(1)}, bf16[256,704]{0,1:T(8,128)(2,1)S(1)}, u32[]{:S(2)}, u32[]{:S(2)}) collective-permute-start(bf16[256,704]{0,1:T(8,128)(2,1)S(1)} %collective-permute-done.2), channel_id=1, source_target_pairs={{0,4},{4,8},{8,12},{12,16},{16,20},{20,24},{24,28},{28,0},{1,5},{5... | collective-permute-start | bytes 1081352 | tf_op jit(solution)/shard_map/ppermute | solution.py:13
  215.9 13.2 %collective-permute-start.5 = (bf16[256,704]{0,1:T(8,128)(2,1)S(1)}, bf16[256,704]{0,1:T(8,128)(2,1)S(1)}, u32[]{:S(2)}, u32[]{:S(2)}) collective-permute-start(bf16[256,704]{0,1:T(8,128)(2,1)S(1)} %collective-permute-done.3), channel_id=1, source_target_pairs={{0,28},{4,0},{8,4},{12,8},{16,12},{20,16},{24,20},{28,24},{1,29},{... | collective-permute-start | bytes 1081352 | tf_op jit(solution)/shard_map/ppermute | solution.py:16
  216.7 17.4 %collective-permute-start.6 = (bf16[256,704]{0,1:T(8,128)(2,1)S(1)}, bf16[256,704]{0,1:T(8,128)(2,1)S(1)}, u32[]{:S(2)}, u32[]{:S(2)}) collective-permute-start(bf16[256,704]{0,1:T(8,128)(2,1)S(1)} %collective-permute-done.4), channel_id=1, source_target_pairs={{0,4},{4,8},{8,12},{12,16},{16,20},{20,24},{24,28},{28,0},{1,5},{5... | collective-permute-start | bytes 1081352 | tf_op jit(solution)/shard_map/ppermute | solution.py:13
  234.9 62.5 %copy-start.7 = (f32[2048]{0:T(1024)S(1)}, f32[2048]{0:T(1024)}, u32[]{:S(2)}) copy-start(f32[2048]{0:T(1024)} %param.29) | copy-start | bytes 24580
  234.9 62.5 %copy-start.9 = (f32[704]{0:T(1024)S(1)}, f32[704]{0:T(1024)}, u32[]{:S(2)}) copy-start(f32[704]{0:T(1024)} %param.34) | copy-start | bytes 8452
Sparse Core Ops, SparseCore 0:
  137.8 33.6 all-reduce.4
  304.5 34.4 all-reduce.6
Sparse Core Ops, SparseCore 1:
  140.3 91.8 all-gather.4
  234.0 63.3 all-gather.6
